TPU v7x, 512 devices: a whole 4x4x16 slice. The times are simulated.
512 devices in a mesh: fs: 64 (over z, y), tp: 8 (over x, core).
Axes of the slice: x: 4, y: 4, z: 16, core: 2. Of those that a mesh axis runs over, the one named last changes fastest.
Arguments:
- saved_inputs: bfloat16 [8192, 4096], P('fs', 'tp'), may hold values from -6 to 6
- value_cotangent: bfloat16 [8192, 2048], P('fs'), may hold values from -0.1875 to 0.1875
- glu_output: bfloat16 [8192, 2048], P('fs', 'tp'), may hold values from -6 to 6
- conv_cotangent: bfloat16 [8192, 2048], P('fs', 'tp'), may hold values from -0.0625 to 0.0625
- factor: bfloat16 [4096, 256], P('tp'), may hold values from -0.09375 to 0.09375
- value_weight: float32 [2048, 4096], P('fs', 'tp'), may hold values from -3 to 3
- first_moment: float32 [2048, 256], P('fs', 'tp'), may hold values from -6 to 6
- second_moment: float32 [2048, 256], P('fs', 'tp'), may hold values from 0.25 to 4
- kernel: float32 [31, 2048], P(None, 'tp'), may hold values from -1 to 1
- kernel_first: float32 [31, 2048], P(None, 'tp'), may hold values from -6 to 6
- kernel_second: float32 [31, 2048], P(None, 'tp'), may hold values from 0.25 to 4
Outputs:
- new_value: float32 [2048, 4096], P('fs', 'tp')
- value_copy: bfloat16 [2048, 4096], P('fs', 'tp')
- value_step: float32 [2048, 4096], P('fs', 'tp')
- new_first: float32 [2048, 256], P('fs', 'tp')
- new_second: float32 [2048, 256], P('fs', 'tp')
- new_kernel: float32 [31, 2048], P(None, 'tp')
- new_kernel_first: float32 [31, 2048], P(None, 'tp')
- new_kernel_second: float32 [31, 2048], P(None, 'tp')
All inputs are finite; a program needn't handle non-finite values.
Results may differ from a plain program's by a relative error of at most 0.0055.
Values may be sent and summed in bfloat16 or wider, within the bound.
A program may use at most 64 MiB of HBM per device.

v0:
```python
import jax
import jax.numpy as jnp
from jax import lax
from jax.sharding import PartitionSpec as P

WIDTH = 4096


def in_blocks(x, dim, peers):
    dims = x.shape
    parts = x.reshape(*dims[:dim], peers, dims[dim] // peers, *dims[dim + 1 :])
    return jnp.moveaxis(parts, dim, 0)


def sum_at_owner(x, axis, dim):
    peers = lax.axis_size(axis)
    parts = lax.all_to_all(in_blocks(x, dim, peers), axis, 0, 0, tiled=True)
    return jnp.sum(parts.astype(jnp.float32), axis=0)


def joined_along(parts, dim):
    parts = jnp.moveaxis(parts, 0, dim)
    dims = parts.shape
    return parts.reshape(*dims[:dim], dims[dim] * dims[dim + 1], *dims[dim + 2 :])


def sent_to_all(x, axis):
    peers = lax.axis_size(axis)
    return lax.all_to_all(jnp.broadcast_to(x[None], (peers, *x.shape)), axis, 0, 0, tiled=True)


def gather_directly(x, axis, dim):
    return joined_along(sent_to_all(x, axis), dim)


def of_everyone(x, axis):
    everything = sent_to_all(x, axis)
    return jnp.sum(everything, axis=0)


def from_behind(x, axis, by):
    peers = lax.axis_size(axis)
    pairs = [(i, i + by) for i in range(peers) if 0 <= i + by < peers]
    return lax.ppermute(x, axis, pairs)


def of_everyone_2(x, axis):
    return sent_to_all(x, axis).astype(jnp.float32).sum(axis=0)


def body(
    saved_inputs,
    value_cotangent,
    glu_output,
    conv_cotangent,
    factor,
    value_weight,
    first_moment,
    second_moment,
    kernel,
    kernel_first,
    kernel_second,
):
    highest = lax.Precision.HIGHEST
    factor_f = factor.astype(jnp.float32)
    partial_reduced = jnp.dot(saved_inputs, factor, preferred_element_type=jnp.float32)
    reduced = sum_at_owner(partial_reduced.astype(jnp.bfloat16), "tp", 1)
    upper_part = reduced.astype(jnp.bfloat16)
    lower_part = (reduced - upper_part.astype(jnp.float32)).astype(jnp.bfloat16)
    dims = (((0,), (0,)), ((), ()))
    upper_term = lax.dot_general(
        value_cotangent, upper_part, dims, preferred_element_type=jnp.float32
    )
    lower_term = lax.dot_general(
        value_cotangent, lower_part, dims, preferred_element_type=jnp.float32
    )
    projected = sum_at_owner((upper_term + lower_term).astype(jnp.bfloat16), "fs", 0)
    new_first = 0.8 * first_moment + 0.2 * projected
    new_second = 0.9 * second_moment + 0.1 * projected * projected
    direction = new_first / jnp.sqrt(new_second)
    full_direction = gather_directly(direction, "tp", 1)
    back_proj = jnp.dot(full_direction, factor_f.T, precision=highest)
    row_squares = of_everyone(jnp.sum(back_proj * back_proj, axis=1), "tp")
    value_step = back_proj / jnp.sqrt(row_squares / WIDTH + 0.01)[:, None]
    new_value = value_weight - 0.05 * value_step
    value_copy = new_value.astype(jnp.bfloat16)
    token_count = glu_output.shape[0]
    reach = kernel.shape[0] - 1
    halo_rows = from_behind(glu_output[token_count - reach :], "fs", 1)
    extended = jnp.concatenate([halo_rows, glu_output], axis=0).astype(jnp.float32)
    cotangent_f = conv_cotangent.astype(jnp.float32)
    pieces = []
    for offset in range(kernel.shape[0]):
        begin = reach - offset
        pieces.append(jnp.sum(extended[begin : begin + token_count] * cotangent_f, axis=0))
    local_grad = jnp.stack(pieces, axis=0)
    kernel_grad = of_everyone_2(local_grad.astype(jnp.bfloat16), "fs").astype(jnp.float32)
    new_kernel_first = 0.8 * kernel_first + 0.2 * kernel_grad
    new_kernel_second = 0.9 * kernel_second + 0.1 * kernel_grad * kernel_grad
    new_kernel = kernel - 0.05 * new_kernel_first / jnp.sqrt(new_kernel_second)
    return (
        new_value,
        value_copy,
        value_step,
        new_first,
        new_second,
        new_kernel,
        new_kernel_first,
        new_kernel_second,
    )


def solution(mesh):
    placed = (
        P("fs", "tp"),
        P("fs", None),
        P("fs", "tp"),
        P("fs", "tp"),
        P("tp", None),
        P("fs", "tp"),
        P("fs", "tp"),
        P("fs", "tp"),
        P(None, "tp"),
        P(None, "tp"),
        P(None, "tp"),
    )
    return jax.shard_map(
        body,
        mesh=mesh,
        in_specs=placed,
        out_specs=(
            P("fs", "tp"),
            P("fs", "tp"),
            P("fs", "tp"),
            P("fs", "tp"),
            P("fs", "tp"),
            P(None, "tp"),
            P(None, "tp"),
            P(None, "tp"),
        ),
        check_vma=False,
    )
```

profile of v0, /device:TPU:16, one launch (start us, length us, event | category | flops | bytes accessed | tf_op | source)
XLA Modules:
  0.0 134.9 jit_solution(4759179826018072566)
XLA Ops:
  0.6 1.3 convolution_convert_fusion
  2.0 9.7 %all_to_all.26 = bf16[8,128,32]{1,2,0:T(8,128)(2,1)S(1)} all-to-all(bf16[8,128,32]{1,2,0:T(8,128)(2,1)S(1)} %bitcast.22), channel_id=1, replica_groups=mesh['fs'=64,'tp'=8] {'tp'}, dimensions={0} | all-to-all | bytes 131072 | tf_op jit(solution)/shard_map/all_to_all | solution.py:17
  13.0 1.1 reshape.320
  14.0 18.6 %all-to-all-start.1 = ((bf16[64,2,512]{2,1,0:T(2,128)(2,1)}), bf16[64,2,512]{2,1,0:T(2,128)(2,1)S(1)}, u32[]{:S(2)}, u32[]{:S(2)}) async-start(bf16[64,2,512]{2,1,0:T(2,128)(2,1)} %reshape.320), calls=%async_computation.1 | async-start | bytes 262144 | tf_op jit(solution)/shard_map/all_to_all | solution.py:17
  32.7 3.1 %collective-permute-start = (bf16[30,256]{1,0:T(8,128)(2,1)S(1)}, bf16[30,256]{1,0:T(8,128)(2,1)S(1)}, u32[]{:S(2)}, u32[]{:S(2)}) collective-permute-start(bf16[30,256]{1,0:T(8,128)(2,1)S(1)} %slice.96), channel_id=1, source_target_pairs={{0,8},{8,16},{16,24},{24,32},{32,40},{40,48},{48,56},{56,64},{64,7... | collective-permute-start | bytes 46088 | tf_op jit(solution)/shard_map/ppermute | solution.py:44
  35.9 2.4 %collective-permute-done = bf16[30,256]{1,0:T(8,128)(2,1)S(1)} collective-permute-done((bf16[30,256]{1,0:T(8,128)(2,1)S(1)}, bf16[30,256]{1,0:T(8,128)(2,1)S(1)}, u32[]{:S(2)}, u32[]{:S(2)}) %collective-permute-start) | collective-permute-done | bytes 15392 | tf_op jit(solution)/shard_map/ppermute | solution.py:44
  38.7 10.2 %all-to-all-done.1 = bf16[64,2,512]{2,1,0:T(2,128)(2,1)S(1)} async-done(((bf16[64,2,512]{2,1,0:T(2,128)(2,1)}), bf16[64,2,512]{2,1,0:T(2,128)(2,1)S(1)}, u32[]{:S(2)}, u32[]{:S(2)}) %all-to-all-start.1) | async-done | bytes 131104 | tf_op jit(solution)/shard_map/all_to_all | solution.py:17
  49.2 0.8 copy.52
  50.4 0.7 reshape.322
  51.1 3.3 %all-to-all-start.2 = ((f32[8,1,1024]{2,1,0:T(1,128)}), f32[8,1,1024]{2,1,0:T(1,128)S(1)}, u32[]{:S(2)}, u32[]{:S(2)}) async-start(f32[8,1,1024]{2,1,0:T(1,128)} %reshape.322), calls=%async_computation.2 | async-start | bytes 65536 | tf_op jit(solution)/shard_map/all_to_all | solution.py:29
  55.0 4.9 %all-to-all-done.2 = f32[8,1,1024]{2,1,0:T(1,128)S(1)} async-done(((f32[8,1,1024]{2,1,0:T(1,128)}), f32[8,1,1024]{2,1,0:T(1,128)S(1)}, u32[]{:S(2)}, u32[]{:S(2)}) %all-to-all-start.2) | async-done | bytes 32800 | tf_op jit(solution)/shard_map/all_to_all | solution.py:29
  59.8 0.5 broadcast.13
  60.3 0.7 reduce.1
  61.8 0.6 broadcast_in_dim.7
  62.4 3.3 %all-to-all-start.3 = ((f32[8,1,32]{2,1,0:T(1,128)}), f32[8,1,32]{2,1,0:T(1,128)S(1)}, u32[]{:S(2)}, u32[]{:S(2)}) async-start(f32[8,1,32]{2,1,0:T(1,128)} %broadcast_in_dim.7), calls=%async_computation.3 | async-start | bytes 8192 | tf_op jit(solution)/shard_map/all_to_all | solution.py:29
  65.9 4.9 %all-to-all-done.3 = f32[8,1,32]{2,1,0:T(1,128)S(1)} async-done(((f32[8,1,32]{2,1,0:T(1,128)}), f32[8,1,32]{2,1,0:T(1,128)S(1)}, u32[]{:S(2)}, u32[]{:S(2)}) %all-to-all-start.3) | async-done | bytes 1056 | tf_op jit(solution)/shard_map/all_to_all | solution.py:29
  70.9 1.1 broadcast_in_dim.8
  72.0 6.0 %all-to-all-start.4 = ((bf16[64,31,256]{2,1,0:T(8,128)(2,1)}), bf16[64,31,256]{2,1,0:T(8,128)(2,1)S(1)}, u32[]{:S(2)}, u32[]{:S(2)}) async-start(bf16[64,31,256]{2,1,0:T(8,128)(2,1)} %broadcast_in_dim.8), calls=%async_computation.4 | async-start | bytes 2097152 | tf_op jit(solution)/shard_map/all_to_all | solution.py:29
  78.0 0.7 copy.59
  78.7 0.7 copy.60
  79.4 0.7 fusion.39
  80.2 53.4 %all-to-all-done.4 = bf16[64,31,256]{2,1,0:T(8,128)(2,1)S(1)} async-done(((bf16[64,31,256]{2,1,0:T(8,128)(2,1)}), bf16[64,31,256]{2,1,0:T(8,128)(2,1)S(1)}, u32[]{:S(2)}, u32[]{:S(2)}) %all-to-all-start.4) | async-done | bytes 1015840 | tf_op jit(solution)/shard_map/all_to_all | solution.py:29
  133.5 0.6 convert_reduce_fusion
  134.2 0.6 multiply_subtract_fusion.1
  (76 shorter events, 3.6 us)
Async XLA Ops:
  0.6 11.1 %copy-start = (bf16[128,2048]{1,0:T(8,128)(2,1)S(1)}, bf16[128,2048]{1,0:T(8,128)(2,1)}, u32[]{:S(2)}) copy-start(bf16[128,2048]{1,0:T(8,128)(2,1)} %param.12) | copy-start | bytes 1572868
  12.6 20.1 %copy-start.3 = (bf16[128,256]{1,0:T(8,128)(2,1)S(1)}, bf16[128,256]{1,0:T(8,128)(2,1)}, u32[]{:S(2)}) copy-start(bf16[128,256]{1,0:T(8,128)(2,1)} %param.13) | copy-start | bytes 196612
  12.6 23.2 %copy-start.8 = (f32[32,32]{1,0:T(8,128)S(1)}, f32[32,32]{1,0:T(8,128)}, u32[]{:S(2)}) copy-start(f32[32,32]{1,0:T(8,128)} %param.17) | copy-start | bytes 12292
  12.6 23.2 %copy-start.9 = (f32[32,32]{1,0:T(8,128)S(1)}, f32[32,32]{1,0:T(8,128)}, u32[]{:S(2)}) copy-start(f32[32,32]{1,0:T(8,128)} %param.18) | copy-start | bytes 12292
  12.6 25.8 %copy-start.2 = (bf16[128,256]{1,0:T(8,128)(2,1)S(1)}, bf16[128,256]{1,0:T(8,128)(2,1)}, u32[]{:S(2)}) copy-start(bf16[128,256]{1,0:T(8,128)(2,1)} %param.14) | copy-start | bytes 196612
  14.0 34.9 %all-to-all-start.1 = ((bf16[64,2,512]{2,1,0:T(2,128)(2,1)}), bf16[64,2,512]{2,1,0:T(2,128)(2,1)S(1)}, u32[]{:S(2)}, u32[]{:S(2)}) async-start(bf16[64,2,512]{2,1,0:T(2,128)(2,1)} %reshape.320), calls=%async_computation.1 | async-start | bytes 262144 | tf_op jit(solution)/shard_map/all_to_all | solution.py:17
  32.7 5.7 %collective-permute-start = (bf16[30,256]{1,0:T(8,128)(2,1)S(1)}, bf16[30,256]{1,0:T(8,128)(2,1)S(1)}, u32[]{:S(2)}, u32[]{:S(2)}) collective-permute-start(bf16[30,256]{1,0:T(8,128)(2,1)S(1)} %slice.96), channel_id=1, source_target_pairs={{0,8},{8,16},{16,24},{24,32},{32,40},{40,48},{48,56},{56,64},{64,7... | collective-permute-start | bytes 46088 | tf_op jit(solution)/shard_map/ppermute | solution.py:44
  51.1 8.7 %all-to-all-start.2 = ((f32[8,1,1024]{2,1,0:T(1,128)}), f32[8,1,1024]{2,1,0:T(1,128)S(1)}, u32[]{:S(2)}, u32[]{:S(2)}) async-start(f32[8,1,1024]{2,1,0:T(1,128)} %reshape.322), calls=%async_computation.2 | async-start | bytes 65536 | tf_op jit(solution)/shard_map/all_to_all | solution.py:29
  54.5 6.9 %copy-start.1 = (bf16[512,256]{1,0:T(8,128)(2,1)S(1)}, bf16[512,256]{1,0:T(8,128)(2,1)}, u32[]{:S(2)}) copy-start(bf16[512,256]{1,0:T(8,128)(2,1)} %param.15) | copy-start | bytes 786436
  62.4 8.5 %all-to-all-start.3 = ((f32[8,1,32]{2,1,0:T(1,128)}), f32[8,1,32]{2,1,0:T(1,128)S(1)}, u32[]{:S(2)}, u32[]{:S(2)}) async-start(f32[8,1,32]{2,1,0:T(1,128)} %broadcast_in_dim.7), calls=%async_computation.3 | async-start | bytes 8192 | tf_op jit(solution)/shard_map/all_to_all | solution.py:29
  72.0 7.4 %copy-start.4 = (f32[32,512]{1,0:T(8,128)S(1)}, f32[32,512]{1,0:T(8,128)}, u32[]{:S(2)}) copy-start(f32[32,512]{1,0:T(8,128)} %param.16) | copy-start | bytes 196612
  72.0 61.6 %all-to-all-start.4 = ((bf16[64,31,256]{2,1,0:T(8,128)(2,1)}), bf16[64,31,256]{2,1,0:T(8,128)(2,1)S(1)}, u32[]{:S(2)}, u32[]{:S(2)}) async-start(bf16[64,31,256]{2,1,0:T(8,128)(2,1)} %broadcast_in_dim.8), calls=%async_computation.4 | async-start | bytes 2097152 | tf_op jit(solution)/shard_map/all_to_all | solution.py:29
  78.0 56.2 %copy-start.5 = (f32[31,256]{1,0:T(8,128)S(1)}, f32[31,256]{1,0:T(8,128)}, u32[]{:S(2)}) copy-start(f32[31,256]{1,0:T(8,128)} %param.19) | copy-start | bytes 95236
  78.0 56.2 %copy-start.6 = (f32[31,256]{1,0:T(8,128)S(1)}, f32[31,256]{1,0:T(8,128)}, u32[]{:S(2)}) copy-start(f32[31,256]{1,0:T(8,128)} %param.20) | copy-start | bytes 95236
  78.0 56.2 %copy-start.7 = (f32[31,256]{1,0:T(8,128)S(1)}, f32[31,256]{1,0:T(8,128)}, u32[]{:S(2)}) copy-start(f32[31,256]{1,0:T(8,128)} %param.21) | copy-start | bytes 95236
where the time goes:
time: 135 us
  waiting for transfers between devices  75.9 us (56%)
  starting transfers between devices  34.3 us (25%)
  blocking collectives  9.72 us (7%)
  local copies, waits for them, and re-layouts  8.17 us (6%)
  other arithmetic  3.52 us (3%)
  matrix products  2.11 us (2%)
    all_to_all x3, waiting for transfers between devices, sent_to_all(): lax.all_to_all(jnp.broadcast_to(x[None], (peers, *x.shape)), axis, 0, 0,...  63.2 us
    all_to_all x1, starting transfers between devices, sum_at_owner(): parts = lax.all_to_all(in_blocks(x, dim, peers), axis, 0, 0, tiled=True)  18.6 us
    all_to_all x3, starting transfers between devices, sent_to_all(): lax.all_to_all(jnp.broadcast_to(x[None], (peers, *x.shape)), axis, 0, 0,...  12.7 us
    all_to_all x1, waiting for transfers between devices, sum_at_owner(): parts = lax.all_to_all(in_blocks(x, dim, peers), axis, 0, 0, tiled=True)  10.2 us
    all_to_all x1, blocking collectives, sum_at_owner(): parts = lax.all_to_all(in_blocks(x, dim, peers), axis, 0, 0, tiled=True)  9.72 us
    unnamed x29, local copies, waits for them, and re-layouts  3.8 us
    ppermute x1, starting transfers between devices, from_behind(): return lax.ppermute(x, axis, pairs)  3.08 us
  transfers between devices with their start and end apart: 5, of which 5 were waited for; matrix products, arithmetic and copies ran while one was open for 2% of the time, Pallas kernels for 0%

commit v1 on v0

v1 whole, which is shorter than its diff:
```python
import functools

import jax
import jax.numpy as jnp
from jax import lax
from jax.experimental import pallas as pl
from jax.experimental.pallas import tpu as pltpu
from jax.sharding import PartitionSpec as P

MESH = pl.DeviceIdType.MESH
F32 = jnp.float32
BF16 = jnp.bfloat16
Y = 4
L = 128
HBM = pl.BlockSpec(memory_space=pltpu.HBM)
VM = pl.BlockSpec(memory_space=pltpu.VMEM)
(P1, HALO, GR, GA, CY, CZ, CA, PY, PZ, P3) = range(10)
MM = (((1,), (0,)), ((), ()))
NT = (((1,), (1,)), ((), ()))


def mm(a, b, dims=MM):
    return lax.dot_general(a, b, dims, preferred_element_type=F32)


def split(x):
    upper = x.astype(BF16)
    return upper, (x - upper.astype(F32)).astype(BF16)


def far_first(n):
    return sorted(range(1, n), key=lambda d: -min(d, n - d))


def comm_kernel(
    Z, TP,
    si_h, vc_h, glu_h, cot_h, fac_h, fm_h, sm_h,
    step_o, nf_o, ns_o, kg_o,
    si, vc, glu, cot, fac, fm, sm,
    p1_s, p1_r, halo, ext, acc, lg, cy_r, cz_s, cz_r, ca,
    g_s, g_r, ga, py_s, py_r, pz_s, pz_r, dirs, rhs, ft3, pad, lhs,
    in_sem, send_sem, recv_sem,
):
    f, t = lax.axis_index("fs"), lax.axis_index("tp")
    z, y = f // Y, lax.rem(f, Y)
    FS = Z * Y
    C = 32
    tp_at = lambda d: {"fs": f, "tp": lax.rem(t + d, TP)}
    y_at = lambda d: {"fs": z * Y + lax.rem(y + d, Y), "tp": t}
    z_at = lambda d: {"fs": lax.rem(z + d, Z) * Y + y, "tp": t}
    f_at = lambda d: {"fs": lax.rem(f + d, FS), "tp": t}

    def send(phase, src, dst, where):
        pltpu.make_async_remote_copy(
            src_ref=src, dst_ref=dst, send_sem=send_sem.at[phase], recv_sem=recv_sem.at[phase],
            device_id=where, device_id_type=MESH,
        ).start()

    def take(sem, like):
        pltpu.make_async_copy(like, like, sem).wait()

    def arrived(phase, like):
        take(recv_sem.at[phase], like)

    loads = []
    for i, (src, dst) in enumerate(
        [(si_h, si), (fac_h, fac), (glu_h, glu), (cot_h, cot), (vc_h, vc), (fm_h, fm), (sm_h, sm)]
    ):
        loads.append(pltpu.make_async_copy(src, dst, in_sem.at[i]))
        loads[-1].start()

    barrier = pltpu.get_barrier_semaphore()
    peers = [z_at(d) for d in far_first(Z)]
    peers += [tp_at(d) for d in range(1, TP)] + [y_at(d) for d in range(1, Y)]
    peers += [f_at(1), f_at(FS - 1)]
    for where in peers:
        pl.semaphore_signal(barrier, inc=1, device_id=where, device_id_type=MESH)

    loads[0].wait()
    loads[1].wait()
    partial = mm(si[...], fac[...]).T
    p1_s[...] = partial.astype(BF16).reshape(p1_s.shape)

    tokens = glu.shape[0]
    CB = ext.shape[0]
    loads[2].wait()
    loads[3].wait()
    pl.semaphore_wait(barrier, len(peers))
    for d in range(1, TP):
        to = lax.rem(t + d, TP)
        send(P1, p1_s.at[to], p1_r.at[d - 1], tp_at(d))
    send(HALO, glu.at[pl.ds(tokens - 32, 32)], halo, f_at(1))

    for c in range(CB):
        ext[c, 32:] = glu[:, c * L : (c + 1) * L].astype(F32)
    late = jnp.stack([cot[32:, c * L : (c + 1) * L].astype(F32) for c in range(CB)])
    for k in range(31):
        prod = ext[:, 64 - k : 32 + tokens - k, :] * late
        acc[:, k] = prod.reshape(CB, (tokens - 32) // 8, 8, L).sum(axis=1)

    flip = fac[...].astype(F32).T
    ft3[...] = flip.reshape(ft3.shape)
    width = fac.shape[0]
    ftp = jnp.concatenate([ft3[:, j].reshape(TP * 8, width) for j in range(4)], axis=0).astype(BF16)
    rhs[:, :width] = ftp
    gram = mm(ftp, ftp, NT)
    g_s[...] = gram.reshape(g_s.shape)
    for d in range(1, TP):
        to = lax.rem(t + d, TP)
        send(GR, g_s.at[to], g_r.at[d - 1], tp_at(d))

    arrived(HALO, halo)
    first = (f > 0).astype(F32)
    for c in range(CB):
        ext[c, :32] = halo[:, c * L : (c + 1) * L].astype(F32) * first
    early = jnp.stack([cot[:32, c * L : (c + 1) * L].astype(F32) for c in range(CB)])
    for k in range(31):
        prod = ext[:, 32 - k : 64 - k, :] * early
        acc[:, k] += prod.reshape(CB, 4, 8, L).sum(axis=1)
    acc[:, 31] = jnp.zeros((CB, 8, L), F32)
    for c in range(CB):
        lg[:, :, c * L : (c + 1) * L] = acc[c].sum(axis=1).reshape(4, 8, L)
    for d in range(1, Y):
        to = lax.rem(y + d, Y)
        send(CY, lg.at[to], cy_r.at[d - 1], y_at(d))

    arrived(P1, p1_r)
    reduced = p1_s[t].astype(F32)
    for d in range(1, TP):
        reduced += p1_r[d - 1].astype(F32)
    lhs2 = jnp.concatenate(split(reduced), axis=0)
    loads[4].wait()
    lane = lax.broadcasted_iota(jnp.int32, (16, L), 1)
    left, even = lane < 64, lax.rem(lane, 64) < 32
    for pair in range(Z // 2):
        both = mm(lhs2, vc[:, pair * 2 * L : (pair + 1) * 2 * L])
        both = both[:C] + both[C:]
        v = [
            jnp.concatenate([both[8 * j : 8 * j + 8, :L], both[8 * j : 8 * j + 8, L:]], axis=0)
            for j in range(4)
        ]
        a = [None] * 4
        for j in range(2):
            a[j] = jnp.where(left, v[j], pltpu.roll(v[j + 2], 64, 1))
            a[j + 2] = jnp.where(left, pltpu.roll(v[j], 64, 1), v[j + 2])
        for h in (0, 2):
            py_s[h, pair * 16 : pair * 16 + 16] = jnp.where(
                even, a[h], pltpu.roll(a[h + 1], 32, 1)
            ).astype(BF16)
            py_s[h + 1, pair * 16 : pair * 16 + 16] = jnp.where(
                even, pltpu.roll(a[h], 96, 1), a[h + 1]
            ).astype(BF16)
    for d in range(1, Y):
        to = lax.rem(y + d, Y)
        send(PY, py_s.at[to], py_r.at[d - 1], y_at(d))

    arrived(CY, cy_r)
    taps = lg[y] + cy_r[0] + cy_r[1] + cy_r[2]
    cz_s[...] = taps.astype(BF16)
    for d in far_first(Z):
        send(CZ, cz_s, cz_r.at[d - 1], z_at(d))

    arrived(GR, g_r)
    rows = g_s[t]
    for d in range(1, TP):
        rows += g_r[d - 1]
    ga[t] = rows
    for d in range(1, TP):
        send(GA, ga.at[t], ga.at[t], tp_at(d))

    arrived(PY, py_r)
    summed = py_s[y].astype(F32)
    for d in range(1, Y):
        summed += py_r[d - 1].astype(F32)
    pz_s[...] = summed.reshape(Z, 8, L).astype(BF16)
    for d in far_first(Z):
        to = lax.rem(z + d, Z)
        send(PZ, pz_s.at[to], pz_r.at[d - 1], z_at(d))

    lanes8 = lax.broadcasted_iota(jnp.int32, (8, L), 1)

    def packed(ref):
        pad[...] = jnp.zeros_like(pad)
        pad[:C, :C] = ref[...]
        flipped = pad[...].T
        out = flipped[:8]
        for j in range(1, 4):
            out += pltpu.roll(flipped[8 * j : 8 * j + 8], 32 * j, 1)
        return out

    def unpacked(x):
        for j in range(4):
            pad[8 * j : 8 * j + 8] = x if j == 0 else pltpu.roll(x, L - 32 * j, 1)
        return pad[...].T[:C, :C]

    loads[5].wait()
    loads[6].wait()
    first_moment = packed(fm)
    second_moment = packed(sm)

    arrived(GA, ga.at[pl.ds(0, TP - 1)])
    upper, lower = split(ga[...].reshape(TP * C, TP * C))
    rhs[:, width : width + TP * C] = upper
    rhs[:, width + TP * C :] = lower

    arrived(CZ, cz_r)
    total = taps
    for d in range(1, Z):
        total += cz_r[d - 1].astype(F32)
    ca[y] = total
    for d in range(1, Y):
        send(CA, ca.at[y], ca.at[y], y_at(d))

    arrived(PZ, pz_r)
    projected = pz_s[z].astype(F32)
    for d in range(1, Z):
        projected += pz_r[d - 1].astype(F32)
    new_first = 0.8 * first_moment + 0.2 * projected
    new_second = 0.9 * second_moment + 0.1 * projected * projected
    dirs[t] = new_first / jnp.sqrt(new_second)
    for d in range(1, TP):
        send(P3, dirs.at[t], dirs.at[t], tp_at(d))

    nf_o[...] = unpacked(new_first)
    ns_o[...] = unpacked(new_second)
    arrived(CA, ca.at[pl.ds(0, Y - 1)])
    kg_o[...] = ca[...].reshape(kg_o.shape)
    pad[...] = jnp.zeros_like(pad)

    arrived(P3, dirs.at[pl.ds(0, TP - 1)])
    pad[: TP * 8] = dirs[...].reshape(TP * 8, L)
    by_row = pad[...].T
    blocks = []
    for j in range(4):
        at = j * TP * 8
        piece = by_row[C * j : C * j + C]
        piece = pltpu.roll(piece, at % L, 1) if at % L else piece
        if at // L < len(blocks):
            blocks[-1] = blocks[-1] + piece
        else:
            blocks.append(piece)
    full = jnp.concatenate(blocks, axis=1)[:, : TP * C]
    upper, lower = split(full)
    lhs[:C] = upper
    lhs[C:] = lower
    out = mm(lhs[...], rhs[...])
    back = out[:C, :width] + out[C:, :width]
    lower_at = width + TP * C
    quad = out[:C, width:lower_at] + out[C:, width:lower_at] + out[:C, lower_at:]
    squares = jnp.sum(quad * full, axis=1, keepdims=True)
    mean = jnp.maximum(squares, 0.0) / (width * TP)
    step_o[...] = back / jnp.sqrt(mean + 0.01)

    for phase, like in [
        (P1, p1_r), (HALO, halo), (GR, g_r), (GA, ga.at[pl.ds(0, TP - 1)]), (CY, cy_r), (CZ, cz_r),
        (CA, ca.at[pl.ds(0, Y - 1)]), (PY, py_r), (PZ, pz_r), (P3, dirs.at[pl.ds(0, TP - 1)]),
    ]:
        take(send_sem.at[phase], like)


def final_kernel(
    step, nf, ns, kg, vw, kern, kf, ks,
    new_value, value_copy, value_step, new_first, new_second, new_kernel, new_kf, new_ks,
):
    value_step[...] = step[...]
    value = vw[...] - 0.05 * step[...]
    new_value[...] = value
    value_copy[...] = value.astype(BF16)
    new_first[...] = nf[...]
    new_second[...] = ns[...]
    grad = kg[: kern.shape[0]]
    first = 0.8 * kf[...] + 0.2 * grad
    second = 0.9 * ks[...] + 0.1 * grad * grad
    new_kf[...] = first
    new_ks[...] = second
    new_kernel[...] = kern[...] - 0.05 * first / jnp.sqrt(second)


def body(Z, TP, si, vc, glu, cot, fac, vw, fm, sm, kern, kf, ks):
    width, rank = fac.shape
    tokens, channels = vc.shape
    chans = glu.shape[1]
    CB = chans // L
    shape = jax.ShapeDtypeStruct
    v = pltpu.VMEM
    step, nf, ns, kg = pl.pallas_call(
        functools.partial(comm_kernel, Z, TP),
        out_shape=[
            shape((32, width), F32), shape((32, 32), F32), shape((32, 32), F32), shape((32, chans), F32),
        ],
        in_specs=[HBM] * 7,
        out_specs=[VM] * 4,
        scratch_shapes=[
            v(si.shape, BF16), v(vc.shape, BF16), v(glu.shape, BF16), v(cot.shape, BF16),
            v(fac.shape, BF16), v((32, 32), F32), v((32, 32), F32),
            v((TP, 32, tokens), BF16),
            v((TP - 1, 32, tokens), BF16),
            v((32, chans), BF16),
            v((CB, 32 + tokens, L), F32),
            v((CB, 32, 8, L), F32),
            v((Y, 8, chans), F32),
            v((Y - 1, 8, chans), F32),
            v((8, chans), BF16),
            v((Z - 1, 8, chans), BF16),
            v((Y, 8, chans), F32),
            v((TP, 32, rank), F32),
            v((TP - 1, 32, rank), F32),
            v((TP, 32, rank), F32),
            v((Y, Z * 8, L), BF16),
            v((Y - 1, Z * 8, L), BF16),
            v((Z, 8, L), BF16),
            v((Z - 1, 8, L), BF16),
            v((TP, 8, L), F32),
            v((rank, width + 2 * rank), BF16),
            v((TP, 4, 8, width), F32),
            v((L, L), F32),
            v((64, rank), BF16),
            pltpu.SemaphoreType.DMA((7,)),
            pltpu.SemaphoreType.DMA((10,)),
            pltpu.SemaphoreType.DMA((10,)),
        ],
        compiler_params=pltpu.CompilerParams(
            collective_id=0, has_side_effects=True, vmem_limit_bytes=24 * 1024 * 1024
        ),
        name="comm",
    )(si, vc, glu, cot, fac, fm, sm)
    return pl.pallas_call(
        final_kernel,
        out_shape=[
            shape(vw.shape, F32), shape(vw.shape, BF16), shape(vw.shape, F32),
            shape(fm.shape, F32), shape(fm.shape, F32),
            shape(kern.shape, F32), shape(kern.shape, F32), shape(kern.shape, F32),
        ],
        in_specs=[VM] * 8,
        out_specs=[VM] * 8,
        compiler_params=pltpu.CompilerParams(vmem_limit_bytes=8 * 1024 * 1024),
        name="final",
    )(step, nf, ns, kg, vw, kern, kf, ks)


def solution(mesh):
    placed = (
        P("fs", "tp"), P("fs", None), P("fs", "tp"), P("fs", "tp"), P("tp", None), P("fs", "tp"),
        P("fs", "tp"), P("fs", "tp"), P(None, "tp"), P(None, "tp"), P(None, "tp"),
    )
    return jax.shard_map(
        functools.partial(body, mesh.shape["fs"] // Y, mesh.shape["tp"]),
        mesh=mesh,
        in_specs=placed,
        out_specs=(P("fs", "tp"),) * 5 + (P(None, "tp"),) * 3,
        check_vma=False,
    )
```

time: 135 us -> 44.6 us (0.33)
  the two profiles are of different devices: /device:TPU:16 before, /device:TPU:1 now
where the time goes in v1:
time: 44.6 us; the launch traced here: 44.1 us
  Pallas kernels  37.4 us (84%)
  local copies, waits for them, and re-layouts  6.01 us (13%)
  between operations  0.7 us (2%)
    pallas_call x1, Pallas kernels, body(): pl.pallas_call(functools.partial(comm_kernel, Z, TP), out_shape=[shape((3...  36.7 us
    unnamed x22, local copies, waits for them, and re-layouts  6.01 us

profile of v1, /device:TPU:1, one launch (start us, length us, event | category | flops | bytes accessed | tf_op | source)
XLA Modules:
  0.0 44.1 jit_solution(17387354760000623714)
XLA Ops:
  0.6 0.0 copy-start
  0.6 1.0 %copy-done = bf16[128,2048]{1,0:T(8,128)(2,1)S(1)} copy-done((bf16[128,2048]{1,0:T(8,128)(2,1)S(1)}, bf16[128,2048]{1,0:T(8,128)(2,1)}, u32[]{:S(2)}) %copy-start) | copy-done | bytes 524312
  1.7 0.0 copy-start.1
  1.7 0.9 %copy-done.1 = bf16[512,256]{1,0:T(8,128)(2,1)S(1)} copy-done((bf16[512,256]{1,0:T(8,128)(2,1)S(1)}, bf16[512,256]{1,0:T(8,128)(2,1)}, u32[]{:S(2)}) %copy-start.1) | copy-done | bytes 262168
  2.6 0.0 copy-start.2
  2.6 0.9 %copy-done.2 = bf16[128,512]{1,0:T(8,128)(2,1)S(1)} copy-done((bf16[128,512]{1,0:T(8,128)(2,1)S(1)}, bf16[128,512]{1,0:T(8,128)(2,1)}, u32[]{:S(2)}) %copy-start.2) | copy-done | bytes 131096
  3.5 0.0 copy-start.3
  3.5 0.8 %copy-done.3 = bf16[128,256]{1,0:T(8,128)(2,1)S(1)} copy-done((bf16[128,256]{1,0:T(8,128)(2,1)S(1)}, bf16[128,256]{1,0:T(8,128)(2,1)}, u32[]{:S(2)}) %copy-start.3) | copy-done | bytes 65560
  4.4 0.0 copy-start.4
  4.4 0.8 %copy-done.4 = bf16[128,256]{1,0:T(8,128)(2,1)S(1)} copy-done((bf16[128,256]{1,0:T(8,128)(2,1)S(1)}, bf16[128,256]{1,0:T(8,128)(2,1)}, u32[]{:S(2)}) %copy-start.4) | copy-done | bytes 65560
  5.2 0.0 copy-start.9
  5.2 0.7 %copy-done.9 = f32[32,32]{1,0:T(8,128)S(1)} copy-done((f32[32,32]{1,0:T(8,128)S(1)}, f32[32,32]{1,0:T(8,128)}, u32[]{:S(2)}) %copy-start.9) | copy-done | bytes 4120
  5.9 0.0 copy-start.10
  5.9 0.7 %copy-done.10 = f32[32,32]{1,0:T(8,128)S(1)} copy-done((f32[32,32]{1,0:T(8,128)S(1)}, f32[32,32]{1,0:T(8,128)}, u32[]{:S(2)}) %copy-start.10) | copy-done | bytes 4120
  6.7 0.0 copy-start.5
  6.7 0.0 copy-start.6
  6.7 0.0 copy-start.7
  6.7 0.0 copy-start.8
  6.7 36.7 %comm.1 = (f32[32,512]{1,0:T(8,128)S(1)}, f32[32,32]{1,0:T(8,128)S(1)}, f32[32,32]{1,0:T(8,128)S(1)}, f32[32,256]{1,0:T(8,128)S(1)}) custom-call(bf16[128,512]{1,0:T(8,128)(2,1)S(1)} %copy-done.2, bf16[128,2048]{1,0:T(8,128)(2,1)S(1)} %copy-done, bf16[128,256]{1,0:T(8,128)(2,1)S(1)} %copy-done.3, bf16[128,256]{1,0:T(8,128)(2,1)S(1)} %copy-done.4, ...), custom_call_target="tpu_custom_call" | custom-call | tf_op jit(solution)/shard_map/comm/pallas_call | solution.py:286
  43.4 0.0 copy-done.5
  43.4 0.0 copy-done.6
  43.4 0.0 copy-done.7
  43.4 0.0 copy-done.8
  43.4 0.7 %final.1 = (f32[32,512]{1,0:T(8,128)}, bf16[32,512]{1,0:T(8,128)(2,1)}, f32[32,512]{1,0:T(8,128)}, f32[32,32]{1,0:T(8,128)}, f32[32,32]{1,0:T(8,128)}, /*index=5...) custom-call(f32[32,512]{1,0:T(8,128)S(1)} %get-tuple-element.12.step, f32[32,32]{1,0:T(8,128)S(1)} %get-tuple-element.13.nf, ...), custom_call_target="tpu_custom_call" | custom-call | tf_op jit(solution)/shard_map/final/pallas_call | solution.py:327
Async XLA Ops:
  0.6 1.0 %copy-start = (bf16[128,2048]{1,0:T(8,128)(2,1)S(1)}, bf16[128,2048]{1,0:T(8,128)(2,1)}, u32[]{:S(2)}) copy-start(bf16[128,2048]{1,0:T(8,128)(2,1)} %vc_h.1) | copy-start | bytes 1572868
  1.7 0.9 %copy-start.1 = (bf16[512,256]{1,0:T(8,128)(2,1)S(1)}, bf16[512,256]{1,0:T(8,128)(2,1)}, u32[]{:S(2)}) copy-start(bf16[512,256]{1,0:T(8,128)(2,1)} %fac_h.1) | copy-start | bytes 786436
  2.6 0.9 %copy-start.2 = (bf16[128,512]{1,0:T(8,128)(2,1)S(1)}, bf16[128,512]{1,0:T(8,128)(2,1)}, u32[]{:S(2)}) copy-start(bf16[128,512]{1,0:T(8,128)(2,1)} %si_h.1) | copy-start | bytes 393220
  3.5 0.8 %copy-start.3 = (bf16[128,256]{1,0:T(8,128)(2,1)S(1)}, bf16[128,256]{1,0:T(8,128)(2,1)}, u32[]{:S(2)}) copy-start(bf16[128,256]{1,0:T(8,128)(2,1)} %glu_h.1) | copy-start | bytes 196612
  4.4 0.8 %copy-start.4 = (bf16[128,256]{1,0:T(8,128)(2,1)S(1)}, bf16[128,256]{1,0:T(8,128)(2,1)}, u32[]{:S(2)}) copy-start(bf16[128,256]{1,0:T(8,128)(2,1)} %cot_h.1) | copy-start | bytes 196612
  5.2 0.7 %copy-start.9 = (f32[32,32]{1,0:T(8,128)S(1)}, f32[32,32]{1,0:T(8,128)}, u32[]{:S(2)}) copy-start(f32[32,32]{1,0:T(8,128)} %fm_h.1) | copy-start | bytes 12292
  5.9 0.7 %copy-start.10 = (f32[32,32]{1,0:T(8,128)S(1)}, f32[32,32]{1,0:T(8,128)}, u32[]{:S(2)}) copy-start(f32[32,32]{1,0:T(8,128)} %sm_h.1) | copy-start | bytes 12292
  6.7 36.7 %copy-start.5 = (f32[32,512]{1,0:T(8,128)S(1)}, f32[32,512]{1,0:T(8,128)}, u32[]{:S(2)}) copy-start(f32[32,512]{1,0:T(8,128)} %vw.1) | copy-start | bytes 196612
  6.7 36.7 %copy-start.6 = (f32[31,256]{1,0:T(8,128)S(1)}, f32[31,256]{1,0:T(8,128)}, u32[]{:S(2)}) copy-start(f32[31,256]{1,0:T(8,128)} %kern.1) | copy-start | bytes 95236
  6.7 36.7 %copy-start.7 = (f32[31,256]{1,0:T(8,128)S(1)}, f32[31,256]{1,0:T(8,128)}, u32[]{:S(2)}) copy-start(f32[31,256]{1,0:T(8,128)} %kf.1) | copy-start | bytes 95236
  6.7 36.7 %copy-start.8 = (f32[31,256]{1,0:T(8,128)S(1)}, f32[31,256]{1,0:T(8,128)}, u32[]{:S(2)}) copy-start(f32[31,256]{1,0:T(8,128)} %ks.1) | copy-start | bytes 95236
